TPU v7x, 32 devices: a whole 2x2x4 slice. The times are simulated.
32 devices in a mesh: sp: 4 (over y, x), tp: 8 (over z, core).
Axes of the slice: x: 2, y: 2, z: 4, core: 2. Of those that a mesh axis runs over, the one named last changes fastest.
Arguments:
- queries: bfloat16 [4096, 1024], P('sp', 'tp'), may hold values from -18 to 18
- keys: bfloat16 [4096, 256], P('sp'), may hold values from -18 to 18
- values: bfloat16 [4096, 256], P('sp'), may hold values from -6 to 6
- sink_logits: float32 [16], P('tp'), may hold values from 3 to 7
- w_out: bfloat16 [1024, 2048], P('tp'), may hold values from -1.5 to 1.5
- residual: bfloat16 [4096, 2048], P(('sp', 'tp')), may hold values from -6 to 6
- norm_gain: float32 [2048], replicated, may hold values from 0.1 to 1.9
- expert_ids: int32 [4096, 4], P('sp'), may hold values from 0 to 15, all different within a row; in each aligned block of 1024 rows (0 to 1023, 1024 to 2047, ...) at most 512 rows name the same one
- expert_weights: float32 [4096, 4], P('sp'), may hold values from 0.1 to 1.5
- w_gate: bfloat16 [32, 768, 2048], P(('sp', 'tp')), may hold values from -0.125 to 0.125
- w_up: bfloat16 [32, 768, 2048], P(('sp', 'tp')), may hold values from -0.125 to 0.125
- w_down: bfloat16 [32, 768, 2048], P(('sp', 'tp')), may hold values from -0.15625 to 0.15625
- shared_gate: bfloat16 [512, 2048], P('tp'), may hold values from -0.125 to 0.125
- shared_up: bfloat16 [512, 2048], P('tp'), may hold values from -0.125 to 0.125
- shared_down: bfloat16 [512, 2048], P('tp'), may hold values from -0.25 to 0.25
Outputs:
- layer_out: bfloat16 [4096, 2048], P(('sp', 'tp'))
Inputs may be any that keep to these rules, and one draw needn't show every extreme that they name: `expert_ids`: each row names 4 different experts; in each aligned block of 1024 rows no expert is named by more than 512 rows.
All inputs are finite; a program needn't handle non-finite values.
Results may differ from a plain program's by a relative error of at most 0.02.
Values may be sent and summed in bfloat16 or wider, within the bound.
No kernel may reach another device: no remote copies, remote signals or barrier semaphores. Data moves between devices by JAX's collectives and lax.ppermute only.
A program may use at most 128 MiB of HBM per device.

v0:
```python
import jax
import jax.numpy as jnp
from jax import lax
from jax.sharding import PartitionSpec as P

HD = 64
GROUP = 4
WINDOW = 128
TOPK = 4


def shifted(block, axis, distance):
    devices = range(lax.axis_size(axis))
    route = [(i - distance, i) for i in devices if i - distance in devices]
    return lax.ppermute(block, axis, route)


def from_partner(x, axis, apart):
    return lax.ppermute(x, axis, [(i, i ^ 1 << apart) for i in range(lax.axis_size(axis))])


def normalize(after_mix, norm_gain):
    values_f = after_mix.astype(jnp.float32)
    scale = lax.rsqrt(jnp.mean(values_f * values_f, axis=-1, keepdims=True) + 1e-06)
    return (values_f * scale * norm_gain).astype(jnp.bfloat16)


def slot_layout(route_ids, expert_count, capacity):
    flat_ids = route_ids.reshape(-1)
    matches = (flat_ids[:, None] == jnp.arange(expert_count, dtype=jnp.int32)[None, :]).astype(
        jnp.int32
    )
    earlier = jnp.cumsum(matches, axis=0) - matches
    order_in = jnp.sum(earlier * matches, axis=1)
    slot_index = flat_ids * capacity + order_in
    owners = jnp.arange(flat_ids.shape[0], dtype=jnp.int32) // TOPK
    slot_owner = jnp.full((expert_count * capacity,), -1, jnp.int32).at[slot_index].set(owners)
    return (slot_index, slot_owner)


def body(
    queries,
    keys,
    values,
    sink_logits,
    w_out,
    residual,
    norm_gain,
    expert_ids,
    expert_weights,
    w_gate,
    w_up,
    w_down,
    shared_gate,
    shared_up,
    shared_down,
):
    tp_count = lax.axis_size("tp")
    sp_count = lax.axis_size("sp")
    seq_rows = queries.shape[0]
    expert_count = sp_count * tp_count // 2
    capacity = max(2, 2 * seq_rows * TOPK // expert_count)
    local_heads = queries.shape[1] // HD
    kv_start = lax.axis_index("tp") * local_heads // GROUP * HD
    key_cols = lax.dynamic_slice_in_dim(keys, kv_start, HD, 1)
    value_cols = lax.dynamic_slice_in_dim(values, kv_start, HD, 1)
    rim_keys, rim_values = shifted(
        (key_cols[seq_rows - WINDOW :], value_cols[seq_rows - WINDOW :]), "sp", 1
    )
    num_blocks = seq_rows // WINDOW
    key_blocks = key_cols.reshape(num_blocks, WINDOW, HD)
    value_blocks = value_cols.reshape(num_blocks, WINDOW, HD)
    keys_ext = jnp.concatenate(
        [jnp.concatenate([rim_keys[None], key_blocks[:-1]], axis=0), key_blocks], axis=1
    )
    values_ext = jnp.concatenate(
        [jnp.concatenate([rim_values[None], value_blocks[:-1]], axis=0), value_blocks], axis=1
    )
    query_blocks = queries.reshape(num_blocks, WINDOW, local_heads, HD)
    scores = jnp.einsum(
        "nqhd,nsd->nhqs", query_blocks, keys_ext, preferred_element_type=jnp.float32
    ) * HD ** (-0.5)
    query_pos = jnp.arange(WINDOW)[:, None] + WINDOW
    key_pos = jnp.arange(2 * WINDOW)[None, :]
    in_band = (key_pos <= query_pos) & (key_pos > query_pos - WINDOW)
    absolute = (
        lax.axis_index("sp") * seq_rows
        + jnp.arange(num_blocks)[:, None, None] * WINDOW
        + key_pos[None]
        - WINDOW
    )
    allowed = in_band[None] & (absolute >= 0)
    scores = jnp.where(allowed[:, None], scores, -jnp.inf)
    sink_col = jnp.broadcast_to(sink_logits[None, :, None, None], scores.shape[:-1] + (1,))
    combined = jnp.concatenate([scores, sink_col], axis=-1)
    row_max = jnp.max(combined, axis=-1, keepdims=True)
    exps = jnp.exp(combined - row_max)
    weights = (exps[..., :-1] / jnp.sum(exps, axis=-1, keepdims=True)).astype(jnp.bfloat16)
    attended = jnp.einsum("nhqs,nsd->nqhd", weights, values_ext, preferred_element_type=jnp.float32)
    attended = attended.astype(jnp.bfloat16).reshape(seq_rows, local_heads * HD)
    head_rows = lax.all_to_all(attended, "tp", split_axis=0, concat_axis=1, tiled=True)
    projected = jnp.dot(
        head_rows,
        lax.all_gather(w_out, "tp", axis=0, tiled=True),
        preferred_element_type=jnp.float32,
    )
    after_mix = (residual.astype(jnp.float32) + projected).astype(jnp.bfloat16)
    normed = normalize(after_mix, norm_gain)
    tp_index = lax.axis_index("tp")
    lanes = tp_count // 2
    lane = tp_index // 2
    keep = tp_index % 2
    half_cap = capacity // 2
    slot_index, slot_owner = slot_layout(expert_ids, expert_count, capacity)
    all_rows = lax.all_gather(normed, "tp", axis=0, tiled=True)
    lane_owner = lax.dynamic_slice_in_dim(slot_owner.reshape(sp_count, lanes, capacity), lane, 1, 1)
    lane_owner = lane_owner.reshape(sp_count * capacity)
    picked = all_rows[jnp.maximum(lane_owner, 0)]
    outgoing = jnp.where((lane_owner >= 0)[:, None], picked, jnp.zeros((), jnp.bfloat16))
    arrived = lax.all_to_all(
        outgoing.reshape(sp_count, capacity, -1), "sp", split_axis=0, concat_axis=0, tiled=True
    )
    arrived = arrived.reshape(sp_count * capacity, -1)
    gate_act = jnp.einsum("td,fd->tf", arrived, w_gate[0], preferred_element_type=jnp.float32)
    up_act = jnp.einsum("td,fd->tf", arrived, w_up[0], preferred_element_type=jnp.float32)
    hidden = (jax.nn.silu(gate_act) * up_act).astype(jnp.bfloat16)
    half_out = jnp.dot(hidden, w_down[0], preferred_element_type=jnp.float32).astype(jnp.bfloat16)
    half_out = half_out.reshape(sp_count, 2, half_cap, -1)
    mine = lax.dynamic_index_in_dim(half_out, keep, 1, keepdims=False)
    other = lax.dynamic_index_in_dim(half_out, 1 - keep, 1, keepdims=False)
    partner = from_partner(other, "tp", 0)
    expert_sum = (mine.astype(jnp.float32) + partner.astype(jnp.float32)).astype(jnp.bfloat16)
    held = lax.all_to_all(expert_sum, "sp", split_axis=0, concat_axis=0, tiled=True).reshape(
        sp_count * half_cap, -1
    )
    route_rank = slot_index.reshape(seq_rows, TOPK) - expert_ids * capacity
    held_here = (expert_ids % lanes == lane) & (route_rank // half_cap == keep)
    position = expert_ids // lanes * half_cap + route_rank % half_cap
    scaled = jnp.where(held_here, expert_weights, jnp.zeros((), expert_weights.dtype))
    shared_gate_act = jnp.einsum(
        "td,fd->tf", all_rows, shared_gate, preferred_element_type=jnp.float32
    )
    shared_up_act = jnp.einsum("td,fd->tf", all_rows, shared_up, preferred_element_type=jnp.float32)
    shared_hidden = (jax.nn.silu(shared_gate_act) * shared_up_act).astype(jnp.bfloat16)
    partial_sum = jnp.dot(shared_hidden, shared_down, preferred_element_type=jnp.float32)
    for route_slot in range(TOPK):
        partial_sum = partial_sum + scaled[:, route_slot : route_slot + 1] * held[
            position[:, route_slot]
        ].astype(jnp.float32)
    moe_sum = lax.psum_scatter(
        partial_sum.astype(jnp.bfloat16), "tp", scatter_dimension=0, tiled=True
    )
    return (after_mix.astype(jnp.float32) + moe_sum.astype(jnp.float32)).astype(jnp.bfloat16)


def solution(mesh):
    return jax.shard_map(
        body,
        mesh=mesh,
        in_specs=(
            P("sp", "tp"),
            P("sp", None),
            P("sp", None),
            P("tp"),
            P("tp", None),
            P(("sp", "tp"), None),
            P(),
            P("sp", None),
            P("sp", None),
            P(("sp", "tp"), None, None),
            P(("sp", "tp"), None, None),
            P(("sp", "tp"), None, None),
            P("tp", None),
            P("tp", None),
            P("tp", None),
        ),
        out_specs=P(("sp", "tp"), None),
        check_vma=False,
    )
```

profile of v0, /device:TPU:0, one launch (start us, length us, event | category | flops | bytes accessed | tf_op | source)
XLA Modules:
  0.0 462.0 jit_solution(13587522794302528692)
XLA Ops:
  6.5 0.7 all-gather.3.cloned.1.call-update
  7.3 0.0 all-gather.5.cloned.1.call-start
  7.3 2.1 constant_dynamic-slice_fusion
  9.4 0.1 copy.67
  9.5 0.6 slice.80
  10.1 5.5 %collective-permute-start.1 = (bf16[128,64]{0,1:T(8,128)(2,1)}, bf16[128,64]{0,1:T(8,128)(2,1)}, u32[]{:S(2)}, u32[]{:S(2)}) collective-permute-start(bf16[128,64]{0,1:T(8,128)(2,1)} %slice.80), channel_id=1, source_target_pairs={{0,8},{8,16},{16,24},{1,9},{9,17},{17,25},{2,10},{10,18},{18,26},{... | collective-permute-start | bytes 49160 | tf_op jit(solution)/shard_map/ppermute | solution.py:15
  15.6 1.1 copy.66
  16.7 3.4 collective-permute-start
  20.1 0.1 add_compare_fusion
  20.2 0.7 copy_bitcast_fusion.2
  21.0 1.0 broadcast_and_fusion
  22.0 0.7 copy_bitcast_fusion.3
  22.7 2.0 reshape.266
  24.7 1.8 fusion.58
  26.5 0.1 broadcast_maximum_fusion
  26.6 0.1 broadcast_in_dim.66
  26.6 0.3 fusion.57
  27.0 1.0 convolution_convert_fusion.1
  28.0 21.9 %all_to_all.29 = bf16[8,128,128]{1,2,0:T(8,128)(2,1)S(1)} all-to-all(bf16[8,128,128]{1,2,0:T(8,128)(2,1)S(1)} %bitcast.99), channel_id=1, replica_groups=mesh['sp'=4,'tp'=8] {'tp'}, dimensions={0} | all-to-all | bytes 524288 | tf_op jit(solution)/shard_map/all_to_all | solution.py:101
  50.0 14.2 %all-gather.3.cloned.1.call-done = bf16[1024,2048]{1,0:T(8,128)(2,1)} async-done(((bf16[128,2048]{1,0:T(8,128)(2,1)}), bf16[1024,2048]{1,0:T(8,128)(2,1)}) %all-gather.3.cloned.1.call-update) | async-done | bytes 4194320 | tf_op jit(solution)/shard_map/all_gather | solution.py:104
  64.2 3.1 multiply_reduce_fusion
  67.3 1.0 copy-done.4
  68.4 0.9 multiply_convert_fusion.1
  69.3 1.1 copy.50
  70.4 1.3 eq.48
  71.7 1.3 eq.44
  73.0 0.7 fusion.45
  73.8 8.3 %reduce-window.6 = s32[16,32,128]{2,1,0:T(8,128)S(1)} reduce-window(s32[16,32,128]{2,1,0:T(8,128)} %fusion.45, s32[]{:T(128)} %constant.127.clone.1), window={size=1x1x128 pad=0_0x0_0x127_0}, to_apply=%region_3.4 | reduce-window | flops 8323072 | bytes 524292 | tf_op jit(solution)/shard_map/reduce-window
  82.1 0.5 slice_reduce_fusion.4
  82.6 0.2 reduce-window.9
  82.8 1.1 copy.57
  83.8 1.4 mul.144
  85.2 0.1 broadcast_add_fusion
  85.3 0.2 fusion.31
  85.6 15.5 %scatter_custom_fusion = s32[8192]{0:T(1024)S(1)} fusion(s32[4096]{0:T(1024)S(1)} %bitcast.103, s32[4096]{0:T(1024)S(1)} %add_select_fusion.4, s32[]{:T(128)} %constant.132.clone.1), kind=kCustom, calls=%fused_computation.110 | custom fusion | bytes 32772 | tf_op jit(solution)/shard_map/scatter | solution.py:37
  101.2 13.8 %all-gather.5.cloned.1.call-done = bf16[1024,2048]{1,0:T(8,128)(2,1)} async-done(((bf16[128,2048]{1,0:T(8,128)(2,1)}), bf16[1024,2048]{1,0:T(8,128)(2,1)}) %all-gather.5.cloned.1.call-update) | async-done | bytes 4194320 | tf_op jit(solution)/shard_map/all_gather | solution.py:115
  115.0 19.0 %gather_fusion = bf16[2048,2048]{1,0:T(8,128)(2,1)} fusion(bf16[1024,2048]{1,0:T(8,128)(2,1)} %all-gather.5.cloned.1.call-done, s32[2048]{0:T(1024)S(1)} %broadcast_clamp_fusion), kind=kCustom, calls=%fused_computation | custom fusion | bytes 16785408 | tf_op jit(solution)/shard_map/gather | solution.py:118
  134.1 7.3 %broadcast_select_fusion = bf16[4,512,2048]{2,1,0:T(8,128)(2,1)} fusion(bf16[4,512,2048]{2,1,0:T(8,128)(2,1)} %bitcast.94, pred[4,512]{1,0:T(4,128)(4,1)S(1)} %bitcast.104), kind=kLoop, calls=%fused_computation.9 | loop fusion | flops 4194304 | bytes 16779264 | tf_op jit(solution)/shard_map/jit(_where)/select_n | solution.py:119
  141.3 5.9 %all-to-all-start.1 = ((bf16[4,512,2048]{2,1,0:T(8,128)(2,1)}), bf16[4,512,2048]{2,1,0:T(8,128)(2,1)}, u32[]{:S(2)}, u32[]{:S(2)}) async-start(bf16[4,512,2048]{2,1,0:T(8,128)(2,1)} %broadcast_select_fusion), calls=%async_computation.1 | async-start | bytes 16777216 | tf_op jit(solution)/shard_map/all_to_all | solution.py:120
  147.2 92.8 %all-to-all-done.1 = bf16[4,512,2048]{2,1,0:T(8,128)(2,1)} async-done(((bf16[4,512,2048]{2,1,0:T(8,128)(2,1)}), bf16[4,512,2048]{2,1,0:T(8,128)(2,1)}, u32[]{:S(2)}, u32[]{:S(2)}) %all-to-all-start.1) | async-done | bytes 8388640 | tf_op jit(solution)/shard_map/all_to_all | solution.py:120
  240.1 11.8 %fusion.4 = f32[2048,768]{1,0:T(8,128)} fusion(bf16[2048,2048]{1,0:T(8,128)(2,1)} %bitcast.16, bf16[1,768,2048]{2,1,0:T(8,128)(2,1)} %param.24), kind=kOutput, calls=%fused_computation.15 | convolution fusion | flops 6442450944 | bytes 17825792 | tf_op jit(solution)/shard_map/td,fd->tf/dot_general | solution.py:124
  251.8 21.3 %convolution_convert_fusion = bf16[2048,2048]{1,0:T(8,128)(2,1)} fusion(f32[2048,768]{1,0:T(8,128)} %fusion.4, bf16[2048,2048]{1,0:T(8,128)(2,1)} %bitcast.16, bf16[1,768,2048]{2,1,0:T(8,128)(2,1)S(1)} %copy-done, bf16[1,768,2048]{2,1,0:T(8,128)(2,1)} %param.25), kind=kOutput, calls=%fused_computation.10 | convolution fusion | flops 12898533376 | bytes 29360128 | tf_op jit(solution)/shard_map/dot_general | solution.py:127
  273.2 4.7 %dynamic-slice_bitcast_fusion = bf16[4,256,2048]{2,1,0:T(8,128)(2,1)} fusion(bf16[4,2,256,2048]{3,2,1,0:T(8,128)(2,1)} %bitcast.95, s32[]{:T(128)S(6)} %select_n.104), kind=kLoop, calls=%fused_computation.12 | loop fusion | bytes 8388612 | tf_op jit(solution)/shard_map/jit(dynamic_index_in_dim)/squeeze | solution.py:130
  277.9 7.5 %collective-permute-done.2 = bf16[4,256,2048]{2,1,0:T(8,128)(2,1)} collective-permute-done((bf16[4,256,2048]{2,1,0:T(8,128)(2,1)}, bf16[4,256,2048]{2,1,0:T(8,128)(2,1)}, u32[]{:S(2)}, u32[]{:S(2)}) %collective-permute-start.2) | collective-permute-done | bytes 4194336 | tf_op jit(solution)/shard_map/ppermute | solution.py:19
  285.4 7.7 %fusion = bf16[4,256,2048]{2,1,0:T(8,128)(2,1)} fusion(bf16[4,256,2048]{2,1,0:T(8,128)(2,1)} %collective-permute-done.2, bf16[4,2,256,2048]{3,2,1,0:T(8,128)(2,1)} %bitcast.96, s32[]{:T(128)S(6)} %select_n.103), kind=kLoop, calls=%fused_computation.7 | loop fusion | flops 8388608 | bytes 12582916 | tf_op jit(solution)/shard_map/convert_element_type | solution.py:132
  293.1 5.1 %all-to-all-start.2 = ((bf16[4,256,2048]{2,1,0:T(8,128)(2,1)}), bf16[4,256,2048]{2,1,0:T(8,128)(2,1)}, u32[]{:S(2)}, u32[]{:S(2)}) async-start(bf16[4,256,2048]{2,1,0:T(8,128)(2,1)} %fusion), calls=%async_computation.2 | async-start | bytes 8388608 | tf_op jit(solution)/shard_map/all_to_all | solution.py:133
  298.2 0.3 reduce-scatter.2.cloned.1.call-start
  298.5 0.5 reduce_sum.34
  299.0 0.3 copy.53
  299.3 0.2 copy.56
  299.6 0.6 fusion.26
  300.2 1.0 slice_reduce_fusion.3
  301.2 0.5 fusion.17
  301.8 1.0 fusion.18
  302.9 1.4 fusion.59
  304.3 8.0 %fusion.12 = f32[1024,2048]{1,0:T(8,128)} fusion(bf16[64,2048]{1,0:T(8,128)(2,1)S(1)} %copy-done.6, bf16[1024,2048]{1,0:T(8,128)(2,1)} %all-gather.5.cloned.1.call-done, bf16[64,2048]{1,0:T(8,128)(2,1)S(1)} %copy-done.7, f32[1024,64]{0,1:T(8,128)S(1)} %fusion.59), kind=kOutput, calls=%fused_computation.33 | convolution fusion | flops 537264128 | bytes 13369344 | tf_op jit(solution)/shard_map/dot_general | solution.py:145
  312.3 33.9 %all-to-all-done.2 = bf16[4,256,2048]{2,1,0:T(8,128)(2,1)} async-done(((bf16[4,256,2048]{2,1,0:T(8,128)(2,1)}), bf16[4,256,2048]{2,1,0:T(8,128)(2,1)}, u32[]{:S(2)}, u32[]{:S(2)}) %all-to-all-start.2) | async-done | bytes 4194336 | tf_op jit(solution)/shard_map/all_to_all | solution.py:133
  346.2 11.8 %gather_fusion.1 = bf16[1024,2048]{1,0:T(8,128)(2,1)} fusion(bf16[1024,2048]{1,0:T(8,128)(2,1)} %bitcast.23, s32[1024]{0:T(1024)S(1)} %get-tuple-element.24), kind=kCustom, calls=%fused_computation.1 | custom fusion | bytes 8392704 | tf_op jit(solution)/shard_map/gather | solution.py:147
  358.0 11.6 %gather_fusion.2 = bf16[1024,2048]{1,0:T(8,128)(2,1)} fusion(bf16[1024,2048]{1,0:T(8,128)(2,1)} %bitcast.23, s32[1024]{0:T(1024)S(1)} %get-tuple-element.23), kind=kCustom, calls=%fused_computation.2 | custom fusion | bytes 8392704 | tf_op jit(solution)/shard_map/gather | solution.py:147
  369.6 11.5 %gather_fusion.3 = bf16[1024,2048]{1,0:T(8,128)(2,1)} fusion(bf16[1024,2048]{1,0:T(8,128)(2,1)} %bitcast.23, s32[1024]{0:T(1024)S(1)} %get-tuple-element.22), kind=kCustom, calls=%fused_computation.3 | custom fusion | bytes 8392704 | tf_op jit(solution)/shard_map/gather | solution.py:147
  381.1 11.6 %gather_fusion.4 = bf16[1024,2048]{1,0:T(8,128)(2,1)} fusion(bf16[1024,2048]{1,0:T(8,128)(2,1)} %bitcast.23, s32[1024]{0:T(1024)S(1)} %get-tuple-element.21), kind=kCustom, calls=%fused_computation.4 | custom fusion | bytes 8392704 | tf_op jit(solution)/shard_map/gather | solution.py:147
  392.7 12.4 %add_convert_fusion = bf16[1024,2048]{1,0:T(8,128)(2,1)} fusion(bf16[1024,2048]{1,0:T(8,128)(2,1)} %gather_fusion.4, bf16[1024,2048]{1,0:T(8,128)(2,1)} %gather_fusion.3, bf16[1024,2048]{1,0:T(8,128)(2,1)} %gather_fusion.2, f32[1024,2048]{1,0:T(8,128)} %fusion.12, bf16[1024,2048]{1,0:T(8,128)(2,1)} %gather_fusion.1, f32[1024]{0:T(1024)S(1)} %get-tuple-element.6, ...), kind=kLoop, calls=%fused_computation.8 | loop fusion | flops 27262976 | bytes 29376512 | tf_op jit(solution)/shard_map/convert_element_type | solution.py:151
  405.1 48.2 %reduce-scatter.2.cloned.1.call-done = bf16[128,2048]{1,0:T(8,128)(2,1)} async-done(((bf16[1024,2048]{1,0:T(8,128)(2,1)}), bf16[128,2048]{1,0:T(8,128)(2,1)}) %reduce-scatter.2.cloned.1.call-update) | async-done | bytes 524304 | tf_op jit(solution)/shard_map/reduce_scatter | solution.py:150
  453.2 2.3 add_convert_fusion.1
  (49 shorter events, 0.3 us)
Async XLA Ops:
  6.5 245.3 %copy-start = (bf16[1,768,2048]{2,1,0:T(8,128)(2,1)S(1)}, bf16[1,768,2048]{2,1,0:T(8,128)(2,1)}, u32[]{:S(2)}) copy-start(bf16[1,768,2048]{2,1,0:T(8,128)(2,1)} %param.26) | copy-start | bytes 9437188
  6.5 57.6 %all-gather.3.cloned.1.call-start = ((), (), s32[]{:S(2)}) async-start(), calls=%async_computation.4 | async-start | bytes 4718592 | tf_op jit(solution)/shard_map/all_gather | solution.py:104
  7.3 107.8 %all-gather.5.cloned.1.call-start = ((), (), s32[]{:S(2)}) async-start(), calls=%async_computation.5 | async-start | bytes 4718592 | tf_op jit(solution)/shard_map/all_gather | solution.py:115
  10.1 14.5 %collective-permute-start.1 = (bf16[128,64]{0,1:T(8,128)(2,1)}, bf16[128,64]{0,1:T(8,128)(2,1)}, u32[]{:S(2)}, u32[]{:S(2)}) collective-permute-start(bf16[128,64]{0,1:T(8,128)(2,1)} %slice.80), channel_id=1, source_target_pairs={{0,8},{8,16},{16,24},{1,9},{9,17},{17,25},{2,10},{10,18},{18,26},{... | collective-permute-start | bytes 49160 | tf_op jit(solution)/shard_map/ppermute | solution.py:15
  16.7 10.3 %collective-permute-start = (bf16[128,64]{0,1:T(8,128)(2,1)S(1)}, bf16[128,64]{0,1:T(8,128)(2,1)}, u32[]{:S(2)}, u32[]{:S(2)}) collective-permute-start(bf16[128,64]{0,1:T(8,128)(2,1)S(1)} %slice.78), channel_id=1, source_target_pairs={{0,8},{8,16},{16,24},{1,9},{9,17},{17,25},{2,10},{10,18},{18,26},{... | collective-permute-start | bytes 49160 | tf_op jit(solution)/shard_map/ppermute | solution.py:15
  22.7 3.8 copy-start.12
  24.7 2.3 copy-start.9
  28.0 40.3 %copy-start.11 = (f32[2048]{0:T(1024)S(1)}, f32[2048]{0:T(1024)}, u32[]{:S(2)}) copy-start(f32[2048]{0:T(1024)} %param.21) | copy-start | bytes 24580
  50.0 19.4 %copy-start.8 = (s32[1024,4]{0,1:T(4,128)S(1)}, s32[1024,4]{0,1:T(4,128)}, u32[]{:S(2)}) copy-start(s32[1024,4]{0,1:T(4,128)} %param.22) | copy-start | bytes 49156
  67.3 1.1 copy-start.4
  141.3 98.7 %all-to-all-start.1 = ((bf16[4,512,2048]{2,1,0:T(8,128)(2,1)}), bf16[4,512,2048]{2,1,0:T(8,128)(2,1)}, u32[]{:S(2)}, u32[]{:S(2)}) async-start(bf16[4,512,2048]{2,1,0:T(8,128)(2,1)} %broadcast_select_fusion), calls=%async_computation.1 | async-start | bytes 16777216 | tf_op jit(solution)/shard_map/all_to_all | solution.py:120
  277.9 7.5 %collective-permute-start.2 = (bf16[4,256,2048]{2,1,0:T(8,128)(2,1)}, bf16[4,256,2048]{2,1,0:T(8,128)(2,1)}, u32[]{:S(2)}, u32[]{:S(2)}) collective-permute-start(bf16[4,256,2048]{2,1,0:T(8,128)(2,1)} %dynamic-slice_bitcast_fusion), channel_id=1, source_target_pairs={{0,1},{1,0},{2,3},{3,2},{4,5},{5,4},{6,7},{7,6},{8,9},{9,8},{10,11... | collective-permute-start | bytes 12582920 | tf_op jit(solution)/shard_map/ppermute | solution.py:19
  293.1 6.2 %copy-start.10 = (f32[1024,4]{0,1:T(4,128)S(1)}, f32[1024,4]{0,1:T(4,128)}, u32[]{:S(2)}) copy-start(f32[1024,4]{0,1:T(4,128)} %param.23) | copy-start | bytes 49156
  293.1 6.4 %copy-start.3 = (s32[1024,4]{1,0:T(8,128)S(1)}, s32[1024,4]{1,0:T(8,128)}, u32[]{:S(2)}) copy-start(s32[1024,4]{1,0:T(8,128)} %copy.50) | copy-start | bytes 49156
  293.1 53.1 %all-to-all-start.2 = ((bf16[4,256,2048]{2,1,0:T(8,128)(2,1)}), bf16[4,256,2048]{2,1,0:T(8,128)(2,1)}, u32[]{:S(2)}, u32[]{:S(2)}) async-start(bf16[4,256,2048]{2,1,0:T(8,128)(2,1)} %fusion), calls=%async_computation.2 | async-start | bytes 8388608 | tf_op jit(solution)/shard_map/all_to_all | solution.py:133
  298.2 155.0 %reduce-scatter.2.cloned.1.call-start = ((), (), s32[]{:S(2)}) async-start(), calls=%async_computation.6 | async-start | bytes 4718592 | tf_op jit(solution)/shard_map/reduce_scatter | solution.py:150
  299.6 3.3 copy-start.2
  299.6 3.3 copy-start.5
  301.8 2.5 copy-start.6
  301.8 2.5 copy-start.7
  392.7 62.8 %copy-start.1 = (bf16[1,768,2048]{2,1,0:T(8,128)(2,1)S(1)}, bf16[1,768,2048]{2,1,0:T(8,128)(2,1)}, u32[]{:S(2)}) copy-start(bf16[1,768,2048]{2,1,0:T(8,128)(2,1)} %param.26) | copy-start | bytes 9437188
Sparse Core Ops, SparseCore 0:
  8.9 55.1 all-gather.2
  69.5 45.5 all-gather.4
  405.2 47.9 reduce-scatter.1
where the time goes:
time: 464 us; the launch traced here: 462 us
  waiting for transfers between devices  211 us (45%)
  local copies, waits for them, and re-layouts  103 us (22%)
  matrix products  48.4 us (10%)
  other arithmetic  43.9 us (9%)
  blocking collectives  21.9 us (5%)
  starting transfers between devices  20.1 us (4%)
  between operations  13.5 us (3%)
    all_to_all x1, waiting for transfers between devices, body(): lax.all_to_all(outgoing.reshape(sp_count, capacity, -1), 'sp', split_axis...  92.8 us
    reduce_scatter x1, waiting for transfers between devices, body(): lax.psum_scatter(partial_sum.astype(jnp.bfloat16), 'tp', scatter_dimensio...  48.2 us
    gather x4, local copies, waits for them, and re-layouts, body(): held[position[:, route_slot]].astype(jnp.float32)  46.5 us
    all_to_all x1, waiting for transfers between devices, body(): lax.all_to_all(expert_sum, 'sp', split_axis=0, concat_axis=0, tiled=True)  33.9 us
    all_to_all x1, blocking collectives, body(): lax.all_to_all(attended, 'tp', split_axis=0, concat_axis=1, tiled=True)  21.9 us
    dot_general x1, matrix products, body(): jnp.dot(hidden, w_down[0], preferred_element_type=jnp.float32)  21.3 us
    gather x1, local copies, waits for them, and re-layouts, body(): picked = all_rows[jnp.maximum(lane_owner, 0)]  19 us
    scatter x1, local copies, waits for them, and re-layouts, slot_layout(): jnp.full((expert_count * capacity,), -1, jnp.int32).at[slot_index]  15.5 us
  transfers between devices with their start and end apart: 8, of which 6 were waited for; matrix products, arithmetic and copies ran while one was open for 12% of the time, Pallas kernels for 0%

commit v1 on v0

--- a/solution.py
+++ b/solution.py
@@ -98,7 +98,10 @@
     weights = (exps[..., :-1] / jnp.sum(exps, axis=-1, keepdims=True)).astype(jnp.bfloat16)
     attended = jnp.einsum("nhqs,nsd->nqhd", weights, values_ext, preferred_element_type=jnp.float32)
     attended = attended.astype(jnp.bfloat16).reshape(seq_rows, local_heads * HD)
-    head_rows = lax.all_to_all(attended, "tp", split_axis=0, concat_axis=1, tiled=True)
+    head_rows = jnp.concatenate(
+        lax.all_to_all(jnp.stack(jnp.split(attended, lax.axis_size("tp"), axis=0)), "tp", 0, 0),
+        axis=1,
+    )
     projected = jnp.dot(
         head_rows,
         lax.all_gather(w_out, "tp", axis=0, tiled=True),

time: 464 us -> 464 us (level)
  no operation moved by 1% of the time
where the time goes in v1:
time: 464 us; the launch traced here: 462 us
  waiting for transfers between devices  211 us (45%)
  local copies, waits for them, and re-layouts  103 us (22%)
  matrix products  48.4 us (10%)
  other arithmetic  43.9 us (9%)
  blocking collectives  21.9 us (5%)
  starting transfers between devices  20.1 us (4%)
  between operations  13.6 us (3%)
    all_to_all x1, waiting for transfers between devices, body(): lax.all_to_all(outgoing.reshape(sp_count, capacity, -1), 'sp', split_axis...  92.8 us
    reduce_scatter x1, waiting for transfers between devices, body(): lax.psum_scatter(partial_sum.astype(jnp.bfloat16), 'tp', scatter_dimensio...  48.2 us
    gather x4, local copies, waits for them, and re-layouts, body(): held[position[:, route_slot]].astype(jnp.float32)  46.5 us
    all_to_all x1, waiting for transfers between devices, body(): lax.all_to_all(expert_sum, 'sp', split_axis=0, concat_axis=0, tiled=True)  33.9 us
    all_to_all x1, blocking collectives, body(): lax.all_to_all(jnp.stack(jnp.split(attended, lax.axis_size('tp'), axis=0)...  21.9 us
    dot_general x1, matrix products, body(): jnp.dot(hidden, w_down[0], preferred_element_type=jnp.float32)  21.3 us
    gather x1, local copies, waits for them, and re-layouts, body(): picked = all_rows[jnp.maximum(lane_owner, 0)]  19 us
    scatter x1, local copies, waits for them, and re-layouts, slot_layout(): jnp.full((expert_count * capacity,), -1, jnp.int32).at[slot_index]  15.5 us
  transfers between devices with their start and end apart: 8, of which 6 were waited for; matrix products, arithmetic and copies ran while one was open for 12% of the time, Pallas kernels for 0%

profile of v1, /device:TPU:0, one launch (start us, length us, event | category | flops | bytes accessed | tf_op | source)
XLA Modules:
  0.0 462.0 jit_solution(2828358751631203110)
XLA Ops:
  6.5 0.7 all-gather.3.cloned.1.call-update
  7.3 0.0 all-gather.5.cloned.1.call-start
  7.3 2.1 constant_dynamic-slice_fusion
  9.4 0.1 copy.67
  9.5 0.6 slice.88
  10.1 5.5 %collective-permute-start.1 = (bf16[128,64]{0,1:T(8,128)(2,1)}, bf16[128,64]{0,1:T(8,128)(2,1)}, u32[]{:S(2)}, u32[]{:S(2)}) collective-permute-start(bf16[128,64]{0,1:T(8,128)(2,1)} %slice.88), channel_id=1, source_target_pairs={{0,8},{8,16},{16,24},{1,9},{9,17},{17,25},{2,10},{10,18},{18,26},{... | collective-permute-start | bytes 49160 | tf_op jit(solution)/shard_map/ppermute | solution.py:15
  15.6 1.1 copy.66
  16.7 3.4 collective-permute-start
  20.1 0.1 add_compare_fusion
  20.2 0.7 copy_bitcast_fusion.2
  21.0 1.0 broadcast_and_fusion
  22.0 0.7 copy_bitcast_fusion.3
  22.7 2.0 reshape.286
  24.7 1.8 fusion.60
  26.5 0.1 broadcast_maximum_fusion
  26.6 0.1 broadcast_in_dim.66
  26.6 0.3 fusion.58
  27.0 1.0 fusion.11
  28.2 21.9 %all_to_all.15 = bf16[8,128,128]{1,2,0:T(8,128)(2,1)S(1)} all-to-all(bf16[8,128,128]{1,2,0:T(8,128)(2,1)S(1)} %constant_dynamic-update-slice_fusion), channel_id=1, replica_groups=mesh['sp'=4,'tp'=8] {'tp'}, dimensions={0} | all-to-all | bytes 524288 | tf_op jit(solution)/shard_map/all_to_all | solution.py:102
  50.1 14.1 %all-gather.3.cloned.1.call-done = bf16[1024,2048]{1,0:T(8,128)(2,1)} async-done(((bf16[128,2048]{1,0:T(8,128)(2,1)}), bf16[1024,2048]{1,0:T(8,128)(2,1)}) %all-gather.3.cloned.1.call-update) | async-done | bytes 4194320 | tf_op jit(solution)/shard_map/all_gather | solution.py:107
  64.2 3.1 multiply_reduce_fusion
  67.3 1.0 copy-done.4
  68.4 0.9 multiply_convert_fusion.1
  69.3 1.1 copy.50
  70.4 1.3 eq.48
  71.7 1.3 eq.44
  73.0 0.7 fusion.46
  73.8 8.3 %reduce-window.6 = s32[16,32,128]{2,1,0:T(8,128)S(1)} reduce-window(s32[16,32,128]{2,1,0:T(8,128)} %fusion.46, s32[]{:T(128)} %constant.127.clone.1), window={size=1x1x128 pad=0_0x0_0x127_0}, to_apply=%region_3.4 | reduce-window | flops 8323072 | bytes 524292 | tf_op jit(solution)/shard_map/reduce-window
  82.1 0.5 slice_reduce_fusion.4
  82.6 0.2 reduce-window.9
  82.8 1.1 copy.57
  83.8 1.4 mul.144
  85.2 0.1 broadcast_add_fusion
  85.3 0.2 fusion.32
  85.6 15.5 %scatter_custom_fusion = s32[8192]{0:T(1024)S(1)} fusion(s32[4096]{0:T(1024)S(1)} %bitcast.117, s32[4096]{0:T(1024)S(1)} %add_select_fusion.4, s32[]{:T(128)} %constant.132.clone.1), kind=kCustom, calls=%fused_computation.119 | custom fusion | bytes 32772 | tf_op jit(solution)/shard_map/scatter | solution.py:37
  101.2 13.8 %all-gather.5.cloned.1.call-done = bf16[1024,2048]{1,0:T(8,128)(2,1)} async-done(((bf16[128,2048]{1,0:T(8,128)(2,1)}), bf16[1024,2048]{1,0:T(8,128)(2,1)}) %all-gather.5.cloned.1.call-update) | async-done | bytes 4194320 | tf_op jit(solution)/shard_map/all_gather | solution.py:118
  115.0 19.0 %gather_fusion = bf16[2048,2048]{1,0:T(8,128)(2,1)} fusion(bf16[1024,2048]{1,0:T(8,128)(2,1)} %all-gather.5.cloned.1.call-done, s32[2048]{0:T(1024)S(1)} %broadcast_clamp_fusion), kind=kCustom, calls=%fused_computation | custom fusion | bytes 16785408 | tf_op jit(solution)/shard_map/gather | solution.py:121
  134.1 7.3 %broadcast_select_fusion = bf16[4,512,2048]{2,1,0:T(8,128)(2,1)} fusion(bf16[4,512,2048]{2,1,0:T(8,128)(2,1)} %bitcast.101, pred[4,512]{1,0:T(4,128)(4,1)S(1)} %bitcast.118), kind=kLoop, calls=%fused_computation.9 | loop fusion | flops 4194304 | bytes 16779264 | tf_op jit(solution)/shard_map/jit(_where)/select_n | solution.py:122
  141.3 5.9 %all-to-all-start.1 = ((bf16[4,512,2048]{2,1,0:T(8,128)(2,1)}), bf16[4,512,2048]{2,1,0:T(8,128)(2,1)}, u32[]{:S(2)}, u32[]{:S(2)}) async-start(bf16[4,512,2048]{2,1,0:T(8,128)(2,1)} %broadcast_select_fusion), calls=%async_computation.1 | async-start | bytes 16777216 | tf_op jit(solution)/shard_map/all_to_all | solution.py:123
  147.2 92.8 %all-to-all-done.1 = bf16[4,512,2048]{2,1,0:T(8,128)(2,1)} async-done(((bf16[4,512,2048]{2,1,0:T(8,128)(2,1)}), bf16[4,512,2048]{2,1,0:T(8,128)(2,1)}, u32[]{:S(2)}, u32[]{:S(2)}) %all-to-all-start.1) | async-done | bytes 8388640 | tf_op jit(solution)/shard_map/all_to_all | solution.py:123
  240.1 11.8 %fusion.4 = f32[2048,768]{1,0:T(8,128)} fusion(bf16[2048,2048]{1,0:T(8,128)(2,1)} %bitcast.23, bf16[1,768,2048]{2,1,0:T(8,128)(2,1)} %param.24), kind=kOutput, calls=%fused_computation.15 | convolution fusion | flops 6442450944 | bytes 17825792 | tf_op jit(solution)/shard_map/td,fd->tf/dot_general | solution.py:127
  251.8 21.3 %convolution_convert_fusion = bf16[2048,2048]{1,0:T(8,128)(2,1)} fusion(f32[2048,768]{1,0:T(8,128)} %fusion.4, bf16[2048,2048]{1,0:T(8,128)(2,1)} %bitcast.23, bf16[1,768,2048]{2,1,0:T(8,128)(2,1)S(1)} %copy-done, bf16[1,768,2048]{2,1,0:T(8,128)(2,1)} %param.25), kind=kOutput, calls=%fused_computation.10 | convolution fusion | flops 12898533376 | bytes 29360128 | tf_op jit(solution)/shard_map/dot_general | solution.py:130
  273.2 4.7 %dynamic-slice_bitcast_fusion = bf16[4,256,2048]{2,1,0:T(8,128)(2,1)} fusion(bf16[4,2,256,2048]{3,2,1,0:T(8,128)(2,1)} %bitcast.102, s32[]{:T(128)S(6)} %select_n.104), kind=kLoop, calls=%fused_computation.12 | loop fusion | bytes 8388612 | tf_op jit(solution)/shard_map/jit(dynamic_index_in_dim)/squeeze | solution.py:133
  277.9 7.5 %collective-permute-done.2 = bf16[4,256,2048]{2,1,0:T(8,128)(2,1)} collective-permute-done((bf16[4,256,2048]{2,1,0:T(8,128)(2,1)}, bf16[4,256,2048]{2,1,0:T(8,128)(2,1)}, u32[]{:S(2)}, u32[]{:S(2)}) %collective-permute-start.2) | collective-permute-done | bytes 4194336 | tf_op jit(solution)/shard_map/ppermute | solution.py:19
  285.4 7.7 %fusion = bf16[4,256,2048]{2,1,0:T(8,128)(2,1)} fusion(bf16[4,256,2048]{2,1,0:T(8,128)(2,1)} %collective-permute-done.2, bf16[4,2,256,2048]{3,2,1,0:T(8,128)(2,1)} %bitcast.103, s32[]{:T(128)S(6)} %select_n.103), kind=kLoop, calls=%fused_computation.7 | loop fusion | flops 8388608 | bytes 12582916 | tf_op jit(solution)/shard_map/convert_element_type | solution.py:135
  293.1 5.1 %all-to-all-start.2 = ((bf16[4,256,2048]{2,1,0:T(8,128)(2,1)}), bf16[4,256,2048]{2,1,0:T(8,128)(2,1)}, u32[]{:S(2)}, u32[]{:S(2)}) async-start(bf16[4,256,2048]{2,1,0:T(8,128)(2,1)} %fusion), calls=%async_computation.2 | async-start | bytes 8388608 | tf_op jit(solution)/shard_map/all_to_all | solution.py:136
  298.2 0.3 reduce-scatter.2.cloned.1.call-start
  298.5 0.5 reduce_sum.34
  299.0 0.3 copy.53
  299.3 0.2 copy.56
  299.6 0.6 fusion.27
  300.2 1.0 slice_reduce_fusion.3
  301.2 0.5 fusion.18
  301.8 1.0 fusion.19
  302.9 1.4 fusion.61
  304.3 8.0 %fusion.13 = f32[1024,2048]{1,0:T(8,128)} fusion(bf16[64,2048]{1,0:T(8,128)(2,1)S(1)} %copy-done.6, bf16[1024,2048]{1,0:T(8,128)(2,1)} %all-gather.5.cloned.1.call-done, bf16[64,2048]{1,0:T(8,128)(2,1)S(1)} %copy-done.7, f32[1024,64]{0,1:T(8,128)S(1)} %fusion.61), kind=kOutput, calls=%fused_computation.34 | convolution fusion | flops 537264128 | bytes 13369344 | tf_op jit(solution)/shard_map/dot_general | solution.py:148
  312.3 33.9 %all-to-all-done.2 = bf16[4,256,2048]{2,1,0:T(8,128)(2,1)} async-done(((bf16[4,256,2048]{2,1,0:T(8,128)(2,1)}), bf16[4,256,2048]{2,1,0:T(8,128)(2,1)}, u32[]{:S(2)}, u32[]{:S(2)}) %all-to-all-start.2) | async-done | bytes 4194336 | tf_op jit(solution)/shard_map/all_to_all | solution.py:136
  346.2 11.8 %gather_fusion.1 = bf16[1024,2048]{1,0:T(8,128)(2,1)} fusion(bf16[1024,2048]{1,0:T(8,128)(2,1)} %bitcast.30, s32[1024]{0:T(1024)S(1)} %get-tuple-element.32), kind=kCustom, calls=%fused_computation.1 | custom fusion | bytes 8392704 | tf_op jit(solution)/shard_map/gather | solution.py:150
  358.0 11.6 %gather_fusion.2 = bf16[1024,2048]{1,0:T(8,128)(2,1)} fusion(bf16[1024,2048]{1,0:T(8,128)(2,1)} %bitcast.30, s32[1024]{0:T(1024)S(1)} %get-tuple-element.31), kind=kCustom, calls=%fused_computation.2 | custom fusion | bytes 8392704 | tf_op jit(solution)/shard_map/gather | solution.py:150
  369.6 11.5 %gather_fusion.3 = bf16[1024,2048]{1,0:T(8,128)(2,1)} fusion(bf16[1024,2048]{1,0:T(8,128)(2,1)} %bitcast.30, s32[1024]{0:T(1024)S(1)} %get-tuple-element.30), kind=kCustom, calls=%fused_computation.3 | custom fusion | bytes 8392704 | tf_op jit(solution)/shard_map/gather | solution.py:150
  381.1 11.6 %gather_fusion.4 = bf16[1024,2048]{1,0:T(8,128)(2,1)} fusion(bf16[1024,2048]{1,0:T(8,128)(2,1)} %bitcast.30, s32[1024]{0:T(1024)S(1)} %get-tuple-element.29), kind=kCustom, calls=%fused_computation.4 | custom fusion | bytes 8392704 | tf_op jit(solution)/shard_map/gather | solution.py:150
  392.7 12.4 %add_convert_fusion = bf16[1024,2048]{1,0:T(8,128)(2,1)} fusion(bf16[1024,2048]{1,0:T(8,128)(2,1)} %gather_fusion.4, bf16[1024,2048]{1,0:T(8,128)(2,1)} %gather_fusion.3, bf16[1024,2048]{1,0:T(8,128)(2,1)} %gather_fusion.2, f32[1024,2048]{1,0:T(8,128)} %fusion.13, bf16[1024,2048]{1,0:T(8,128)(2,1)} %gather_fusion.1, f32[1024]{0:T(1024)S(1)} %get-tuple-element.6, ...), kind=kLoop, calls=%fused_computation.8 | loop fusion | flops 27262976 | bytes 29376512 | tf_op jit(solution)/shard_map/convert_element_type | solution.py:154
  405.1 48.2 %reduce-scatter.2.cloned.1.call-done = bf16[128,2048]{1,0:T(8,128)(2,1)} async-done(((bf16[1024,2048]{1,0:T(8,128)(2,1)}), bf16[128,2048]{1,0:T(8,128)(2,1)}) %reduce-scatter.2.cloned.1.call-update) | async-done | bytes 524304 | tf_op jit(solution)/shard_map/reduce_scatter | solution.py:153
  453.2 2.3 add_convert_fusion.1
  (58 shorter events, 0.4 us)
Async XLA Ops:
  6.5 245.3 %copy-start = (bf16[1,768,2048]{2,1,0:T(8,128)(2,1)S(1)}, bf16[1,768,2048]{2,1,0:T(8,128)(2,1)}, u32[]{:S(2)}) copy-start(bf16[1,768,2048]{2,1,0:T(8,128)(2,1)} %param.26) | copy-start | bytes 9437188
  6.5 57.6 %all-gather.3.cloned.1.call-start = ((), (), s32[]{:S(2)}) async-start(), calls=%async_computation.4 | async-start | bytes 4718592 | tf_op jit(solution)/shard_map/all_gather | solution.py:107
  7.3 107.8 %all-gather.5.cloned.1.call-start = ((), (), s32[]{:S(2)}) async-start(), calls=%async_computation.5 | async-start | bytes 4718592 | tf_op jit(solution)/shard_map/all_gather | solution.py:118
  10.1 14.5 %collective-permute-start.1 = (bf16[128,64]{0,1:T(8,128)(2,1)}, bf16[128,64]{0,1:T(8,128)(2,1)}, u32[]{:S(2)}, u32[]{:S(2)}) collective-permute-start(bf16[128,64]{0,1:T(8,128)(2,1)} %slice.88), channel_id=1, source_target_pairs={{0,8},{8,16},{16,24},{1,9},{9,17},{17,25},{2,10},{10,18},{18,26},{... | collective-permute-start | bytes 49160 | tf_op jit(solution)/shard_map/ppermute | solution.py:15
  16.7 10.3 %collective-permute-start = (bf16[128,64]{0,1:T(8,128)(2,1)S(1)}, bf16[128,64]{0,1:T(8,128)(2,1)}, u32[]{:S(2)}, u32[]{:S(2)}) collective-permute-start(bf16[128,64]{0,1:T(8,128)(2,1)S(1)} %slice.86), channel_id=1, source_target_pairs={{0,8},{8,16},{16,24},{1,9},{9,17},{17,25},{2,10},{10,18},{18,26},{... | collective-permute-start | bytes 49160 | tf_op jit(solution)/shard_map/ppermute | solution.py:15
  22.7 3.8 copy-start.12
  24.7 2.3 copy-start.9
  28.0 40.3 %copy-start.11 = (f32[2048]{0:T(1024)S(1)}, f32[2048]{0:T(1024)}, u32[]{:S(2)}) copy-start(f32[2048]{0:T(1024)} %param.21) | copy-start | bytes 24580
  50.1 19.2 %copy-start.8 = (s32[1024,4]{0,1:T(4,128)S(1)}, s32[1024,4]{0,1:T(4,128)}, u32[]{:S(2)}) copy-start(s32[1024,4]{0,1:T(4,128)} %param.22) | copy-start | bytes 49156
  67.3 1.1 copy-start.4
  141.3 98.7 %all-to-all-start.1 = ((bf16[4,512,2048]{2,1,0:T(8,128)(2,1)}), bf16[4,512,2048]{2,1,0:T(8,128)(2,1)}, u32[]{:S(2)}, u32[]{:S(2)}) async-start(bf16[4,512,2048]{2,1,0:T(8,128)(2,1)} %broadcast_select_fusion), calls=%async_computation.1 | async-start | bytes 16777216 | tf_op jit(solution)/shard_map/all_to_all | solution.py:123
  277.9 7.5 %collective-permute-start.2 = (bf16[4,256,2048]{2,1,0:T(8,128)(2,1)}, bf16[4,256,2048]{2,1,0:T(8,128)(2,1)}, u32[]{:S(2)}, u32[]{:S(2)}) collective-permute-start(bf16[4,256,2048]{2,1,0:T(8,128)(2,1)} %dynamic-slice_bitcast_fusion), channel_id=1, source_target_pairs={{0,1},{1,0},{2,3},{3,2},{4,5},{5,4},{6,7},{7,6},{8,9},{9,8},{10,11... | collective-permute-start | bytes 12582920 | tf_op jit(solution)/shard_map/ppermute | solution.py:19
  293.1 6.2 %copy-start.10 = (f32[1024,4]{0,1:T(4,128)S(1)}, f32[1024,4]{0,1:T(4,128)}, u32[]{:S(2)}) copy-start(f32[1024,4]{0,1:T(4,128)} %param.23) | copy-start | bytes 49156
  293.1 6.4 %copy-start.3 = (s32[1024,4]{1,0:T(8,128)S(1)}, s32[1024,4]{1,0:T(8,128)}, u32[]{:S(2)}) copy-start(s32[1024,4]{1,0:T(8,128)} %copy.50) | copy-start | bytes 49156
  293.1 53.1 %all-to-all-start.2 = ((bf16[4,256,2048]{2,1,0:T(8,128)(2,1)}), bf16[4,256,2048]{2,1,0:T(8,128)(2,1)}, u32[]{:S(2)}, u32[]{:S(2)}) async-start(bf16[4,256,2048]{2,1,0:T(8,128)(2,1)} %fusion), calls=%async_computation.2 | async-start | bytes 8388608 | tf_op jit(solution)/shard_map/all_to_all | solution.py:136
  298.2 155.0 %reduce-scatter.2.cloned.1.call-start = ((), (), s32[]{:S(2)}) async-start(), calls=%async_computation.6 | async-start | bytes 4718592 | tf_op jit(solution)/shard_map/reduce_scatter | solution.py:153
  299.6 3.3 copy-start.2
  299.6 3.3 copy-start.5
  301.8 2.5 copy-start.6
  301.8 2.5 copy-start.7
  392.7 62.8 %copy-start.1 = (bf16[1,768,2048]{2,1,0:T(8,128)(2,1)S(1)}, bf16[1,768,2048]{2,1,0:T(8,128)(2,1)}, u32[]{:S(2)}) copy-start(bf16[1,768,2048]{2,1,0:T(8,128)(2,1)} %param.26) | copy-start | bytes 9437188
Sparse Core Ops, SparseCore 0:
  8.9 55.1 all-gather.2
  69.5 45.5 all-gather.4
  405.2 47.9 reduce-scatter.1
